TPU v7x, 128 devices: a whole 4x4x4 slice. The times are simulated.
128 devices in a mesh: rep: 16 (over z, x), fs: 4 (over y), tp: 2 (over core).
Axes of the slice: x: 4, y: 4, z: 4, core: 2. Of those that a mesh axis runs over, the one named last changes fastest.
Arguments:
- inputs: bfloat16 [64, 768, 2048], P(('rep', 'fs'), 'tp'), may hold values from -6 to 6
- pre_gate: bfloat16 [64, 768, 2816], P(('rep', 'fs'), None, 'tp'), may hold values from -6 to 6
- pre_up: bfloat16 [64, 768, 2816], P(('rep', 'fs'), None, 'tp'), may hold values from -6 to 6
- cotangent: bfloat16 [64, 768, 2816], P(('rep', 'fs'), None, 'tp'), may hold values from -16 to 16
- w_gate: bfloat16 [2048, 2816], P('fs', 'tp'), may hold values from -0.125 to 0.125
- w_up: bfloat16 [2048, 2816], P('fs', 'tp'), may hold values from -0.125 to 0.125
- taps_gate: bfloat16 [3, 2816], replicated, may hold values from -3 to 3
- taps_up: bfloat16 [3, 2816], replicated, may hold values from -3 to 3
Outputs:
- grad_inputs: bfloat16 [64, 768, 2048], P(('rep', 'fs'), 'tp')
- grad_w_gate: float32 [2048, 2816], P('fs', 'tp')
- grad_w_up: float32 [2048, 2816], P('fs', 'tp')
- grad_taps_gate: float32 [3, 2816], replicated
- grad_taps_up: float32 [3, 2816], replicated
All inputs are finite; a program needn't handle non-finite values.
Results may differ from a plain program's by a relative error of at most 0.0059.
Values may be sent and summed in bfloat16 or wider, within the bound.
No kernel may reach another device: no remote copies, remote signals or barrier semaphores. Data moves between devices by JAX's collectives and lax.ppermute only.
A program may use at most 192 MiB of HBM per device.

v0:
```python
import jax
import jax.numpy as jnp
from jax import lax
from jax.sharding import PartitionSpec as P


def laid_out(parts, dim):
    lengths = list(parts.shape[1:])
    lengths[dim] *= parts.shape[0]
    return jnp.moveaxis(parts, 0, dim).reshape(lengths)


def work_in_pieces(x, axis, dim, apply, out_dim):
    size, width = (lax.axis_size(axis), x.shape[dim])
    count = 2 if width % 2 == 0 else 1
    gathered, length = ([], width // count)
    for k in range(count):
        section = lax.slice_in_dim(x, k * length, (k + 1) * length, axis=dim)
        starts = jnp.arange(size) * width + k * length
        gathered.append(jax.vmap(apply)(lax.all_gather(section, axis), starts))
    return laid_out(jnp.concatenate(gathered, axis=out_dim + 1), out_dim)


def split_up(x, dim, count):
    before, after = (x.shape[:dim], x.shape[dim + 1 :])
    return jnp.moveaxis(x.reshape(*before, count, -1, *after), dim, 0)


def sum_at_owner(x, axis, dim):
    count = lax.axis_size(axis)
    parts = lax.all_to_all(split_up(x, dim, count), axis, 0, 0, tiled=True)
    return jnp.sum(parts.astype(jnp.float32), axis=0)


def side_by_side(arrays, axis, dim, along):
    widths = [a.shape[along] for a in arrays]
    both = jnp.concatenate(arrays, axis=along)
    result = lax.psum_scatter(both, axis, scatter_dimension=dim, tiled=True)
    return tuple(jnp.split(result, [sum(widths[:k]) for k in range(1, len(widths))], axis=along))


def in_one(arrays, axis):
    ravelled, at, gathered = (jnp.concatenate([a.reshape(-1) for a in arrays]), 0, [])
    subtotal = lax.psum(ravelled, axis)
    for a in arrays:
        gathered.append(subtotal[at : at + a.size].reshape(a.shape))
        at += a.size
    return tuple(gathered)


def causal_mix(signal, kernel):
    length = signal.shape[0]
    padded = jnp.pad(signal, ((2, 0), (0, 0)))
    return (
        kernel[0] * padded[0:length]
        + kernel[1] * padded[1 : length + 1]
        + kernel[2] * padded[2 : length + 2]
    )


def gated_hidden(gate_pre, up_pre, kernel_gate, kernel_up):
    return jax.nn.gelu(causal_mix(gate_pre, kernel_gate)) * causal_mix(up_pre, kernel_up)


def per_device(inputs, pre_gate, pre_up, cotangent, w_gate, w_up, taps_gate, taps_up):
    columns = pre_gate.shape[2]
    offset = lax.axis_index("tp") * columns
    kernel_gate = lax.dynamic_slice_in_dim(taps_gate, offset, columns, 1).astype(jnp.float32)
    kernel_up = lax.dynamic_slice_in_dim(taps_up, offset, columns, 1).astype(jnp.float32)
    _, pullback = jax.vjp(
        gated_hidden,
        pre_gate[0].astype(jnp.float32),
        pre_up[0].astype(jnp.float32),
        kernel_gate,
        kernel_up,
    )
    back_gate, back_up, tap_gate, tap_up = pullback(cotangent[0].astype(jnp.float32))
    stacked = jnp.stack([back_gate, back_up], axis=1).astype(jnp.bfloat16)
    weights = jnp.stack([w_gate, w_up])

    def project(weight_block, row_start):
        return jnp.einsum("lkf,knf->ln", stacked, weight_block, preferred_element_type=jnp.float32)

    partial_value = work_in_pieces(weights, "fs", 1, project, 1)
    grad_inputs = sum_at_owner(partial_value.astype(jnp.bfloat16), "tp", 0).astype(jnp.bfloat16)[
        None
    ]
    rep_count = lax.axis_size("rep")
    shard_count = lax.axis_size("fs")
    features = inputs.shape[2]
    layout = (shard_count, features // shard_count)
    pattern = "nfd,nk->fdk"
    token_block = lax.all_gather(inputs, "tp", axis=1, tiled=True)
    row_count = token_block.shape[1]
    spread = token_block[0].reshape((row_count,) + layout)
    gate_total = jnp.einsum(pattern, spread, stacked[:, 0], preferred_element_type=jnp.float32)
    up_total = jnp.einsum(pattern, spread, stacked[:, 1], preferred_element_type=jnp.float32)
    factor = float(pre_gate.shape[1] * rep_count * shard_count) ** (-0.5)
    pieces = side_by_side((gate_total, up_total), "fs", 0, 1)
    whole = lax.psum((pieces[0], pieces[1]), "rep")
    grad_w_gate = whole[0].reshape(features // shard_count, columns) * factor
    grad_w_up = whole[1].reshape(features // shard_count, columns) * factor
    blank = jnp.zeros(taps_gate.shape, jnp.float32)
    full_gate = lax.dynamic_update_slice_in_dim(blank, tap_gate, offset, 1)
    full_up = lax.dynamic_update_slice_in_dim(blank, tap_up, offset, 1)
    summed_gate, summed_up = in_one((full_gate, full_up), ("rep", "fs", "tp"))
    return (grad_inputs, grad_w_gate, grad_w_up, summed_gate * factor, summed_up * factor)


def solution(mesh):
    placed = (
        P(("rep", "fs"), "tp", None),
        P(("rep", "fs"), None, "tp"),
        P(("rep", "fs"), None, "tp"),
        P(("rep", "fs"), None, "tp"),
        P("fs", "tp"),
        P("fs", "tp"),
        P(),
        P(),
    )
    return jax.shard_map(
        per_device,
        mesh=mesh,
        in_specs=placed,
        out_specs=(P(("rep", "fs"), "tp", None), P("fs", "tp"), P("fs", "tp"), P(), P()),
        check_vma=False,
    )
```

profile of v0, /device:TPU:1, one launch (start us, length us, event | category | flops | bytes accessed | tf_op | source)
XLA Modules:
  0.0 535.5 jit_solution(3696512987416850347)
XLA Ops:
  8.0 0.0 all-gather.6.cloned.1.call-start
  8.0 0.7 all-gather.6.cloned.1.call-update
  8.7 0.0 reduce-scatter.2.cloned.1.call-start
  8.8 0.7 dynamic-slice_convert_fusion
  9.6 0.1 slice_reduce_fusion.5
  9.6 0.0 copy-start
  9.6 0.0 copy-start.2
  9.6 3.0 bitcast_convert_fusion.2
  12.6 0.0 copy-done
  12.6 0.6 copy-done.2
  13.2 0.0 copy-start.1
  13.2 7.1 %multiply_reduce_fusion.4 = (f32[1408]{0:T(1024)S(1)}, f32[1408]{0:T(1024)S(1)}, f32[1408]{0:T(1024)S(1)}, f32[768,1408]{1,0:T(8,128)S(1)}, f32[768,1408]{1,0:T(8,128)S(1)}) fusion(f32[768,1408]{1,0:T(8,128)S(1)} %get-tuple-element.41, bf16[1,768,1408]{2,1,0:T(8,128)(2,1)S(1)} %copy-done, f32[768,1408]{1,0:T(8,128)S(1)} %get-tuple-element.42, ...), kind=kLoop, calls=%fused_computation.24 | loop fusion | flops 41086848 | bytes 21677568 | tf_op jit(solution)/shard_map/transpose(jvp())/reduce_sum | solution.py:56
  20.3 0.0 copy-done.1
  20.3 4.6 multiply_reduce_fusion.1
  25.0 2.8 broadcast_multiply_fusion.2
  27.8 4.8 fusion.6
  32.6 0.8 broadcast_multiply_fusion.5
  33.4 2.3 fusion.7
  35.8 0.0 all-gather.6.cloned.1.call-done
  35.8 3.4 copy.16
  39.2 0.0 copy-start.5
  39.2 7.3 %convolution_bitcast_fusion = f32[4,512,1408]{2,1,0:T(8,128)S(1)} fusion(bf16[768,4,512]{0,2,1:T(8,128)(2,1)S(1)} %bitcast.73, bf16[768,1408]{1,0:T(8,128)(2,1)} %fusion.6), kind=kOutput, calls=%fused_computation.1 | convolution fusion | flops 4429185024 | bytes 16842752 | tf_op jit(solution)/shard_map/nfd,nk->fdk/dot_general | solution.py:97
  46.5 0.0 copy-done.5
  46.5 5.5 %convolution_bitcast_fusion.1 = f32[4,512,1408]{2,1,0:T(8,128)S(1)} fusion(bf16[768,4,512]{0,2,1:T(8,128)(2,1)S(1)} %bitcast.74, bf16[768,1408]{1,0:T(8,128)(2,1)S(1)} %copy-done.5), kind=kOutput, calls=%fused_computation.2 | convolution fusion | flops 4429185024 | bytes 16842752 | tf_op jit(solution)/shard_map/nfd,nk->fdk/dot_general | solution.py:96
  52.0 9.1 %pad_maximum_fusion = f32[4,1024,1408]{2,1,0:T(8,128)} fusion(f32[4,512,1408]{2,1,0:T(8,128)S(1)} %convolution_bitcast_fusion, f32[4,512,1408]{2,1,0:T(8,128)S(1)} %convolution_bitcast_fusion.1), kind=kLoop, calls=%fused_computation | loop fusion | flops 5767168 | bytes 46137344 | tf_op jit(solution)/shard_map/concatenate | solution.py:37
  61.1 0.0 copy-start.7
  61.1 0.0 copy-start.8
  61.1 0.0 reduce-scatter.2.cloned.1.call-update
  61.2 0.0 all-reduce.18.cloned.1.call-start
  61.4 0.6 pad_maximum_fusion.2
  62.1 0.0 all-reduce.18.cloned.1.call-update
  62.1 0.0 all-gather.10.cloned.1.call-start
  62.2 0.4 copy-done.7
  62.5 0.4 copy-done.8
  62.9 1.8 fusion.14
  64.7 0.0 all-gather.10.cloned.1.call-update
  64.8 0.0 all-gather.8.cloned.1.call-start
  64.8 0.5 all-gather.8.cloned.1.call-update
  65.3 0.3 all-reduce.20.cloned.1.call-start
  65.6 198.4 %reduce-scatter.2.cloned.1.call-done = f32[1,1024,1408]{2,1,0:T(8,128)} async-done(((f32[4,1024,1408]{2,1,0:T(8,128)}), f32[1,1024,1408]{2,1,0:T(8,128)}) %reduce-scatter.2.cloned.1.call-update) | async-done | bytes 5767184 | tf_op jit(solution)/shard_map/reduce_scatter | solution.py:38
  264.0 5.6 %fusion.18 = (f32[1,512,1408]{2,1,0:T(8,128)}, f32[1,512,1408]{2,1,0:T(8,128)}) fusion(f32[1,1024,1408]{2,1,0:T(8,128)} %reduce-scatter.2.cloned.1.call-done), kind=kLoop, calls=%fused_computation.69 | loop fusion | bytes 11534336 | tf_op jit(solution)/shard_map/split | solution.py:39
  269.6 0.0 copy-start.4
  269.6 0.0 all-reduce.20.cloned.1.call-update
  269.6 134.9 %all-reduce.18.cloned.1.call-done = f32[16896]{0:T(1024)} async-done(((f32[16896]{0:T(1024)}), f32[16896]{0:T(1024)}) %all-reduce.18.cloned.1.call-update) | async-done | bytes 67600 | tf_op jit(solution)/shard_map/psum | solution.py:44
  404.5 0.9 slice_multiply_fusion
  405.4 0.6 mul.244
  406.0 0.6 mul.246
  406.6 0.0 copy-done.4
  406.6 9.1 %fusion.13 = bf16[4,768,256]{1,2,0:T(8,128)(2,1)} fusion(bf16[4,2,256,1408]{3,2,1,0:T(8,128)(2,1)} %bitcast.81, bf16[768,1,1408]{2,0,1:T(8,128)(2,1)S(1)} %bitcast.75, bf16[768,1,1408]{2,0,1:T(8,128)(2,1)} %bitcast.77), kind=kOutput, calls=%fused_computation.51 | convolution fusion | flops 4438622208 | bytes 11665408 | tf_op jit(solution)/shard_map/vmap(lkf,knf->ln)/dot_general | solution.py:82
  415.7 0.0 all-gather.8.cloned.1.call-done
  415.7 0.0 copy-start.6
  415.7 8.1 %fusion.12 = bf16[4,768,256]{1,2,0:T(8,128)(2,1)S(1)} fusion(bf16[4,2,256,1408]{3,2,1,0:T(8,128)(2,1)} %bitcast.82, bf16[768,1,1408]{2,0,1:T(8,128)(2,1)S(1)} %bitcast.76, bf16[768,1,1408]{2,0,1:T(8,128)(2,1)} %bitcast.78), kind=kOutput, calls=%fused_computation.50 | convolution fusion | flops 4438622208 | bytes 11665408 | tf_op jit(solution)/shard_map/vmap(lkf,knf->ln)/dot_general | solution.py:82
  423.8 0.0 copy-done.6
  423.8 0.2 maximum_bitcast_fusion.1
  424.0 2.4 convert_element_type.47
  426.5 2.3 copy.14
  428.8 5.9 %all_to_all.5 = bf16[2,384,2048]{1,2,0:T(8,128)(2,1)S(1)} all-to-all(bf16[2,384,2048]{1,2,0:T(8,128)(2,1)S(1)} %copy.14), channel_id=1, replica_groups=mesh['rep'=16,'fs'=4,'tp'=2] {'tp'}, dimensions={0} | all-to-all | bytes 6291456 | tf_op jit(solution)/shard_map/all_to_all | solution.py:31
  434.7 2.2 reduce_sum.65
  436.8 2.6 copy.17
  439.4 83.4 %all-reduce.20.cloned.1.call-done = (f32[1,512,1408]{2,1,0:T(8,128)}, f32[1,512,1408]{2,1,0:T(8,128)}) async-done(((f32[1,512,1408]{2,1,0:T(8,128)}, f32[1,512,1408]{2,1,0:T(8,128)}), (f32[1,512,1408]{2,1,0:T(8,128)}, f32[1,512,1408]{2,1,0:T(8,128)})) %all-reduce.20.cloned.1.call-update) | async-done | bytes 5767184 | tf_op jit(solution)/shard_map/psum | solution.py:100
  522.8 0.0 copy-start.3
  522.8 3.8 multiply_bitcast_fusion.1
  526.6 0.0 copy-done.3
  526.6 1.8 multiply_bitcast_fusion
  (14 shorter events, 0.2 us)
Async XLA Ops:
  8.0 27.8 %all-gather.6.cloned.1.call-start = ((), (), s32[]{:S(2)}) async-start(), calls=%async_computation.2 | async-start | bytes 4718592 | tf_op jit(solution)/shard_map/all_gather | solution.py:93
  8.7 255.2 %reduce-scatter.2.cloned.1.call-start = ((), (), s32[]{:S(2)}) async-start(), calls=%async_computation.3 | async-start | bytes 28835840 | tf_op jit(solution)/shard_map/reduce_scatter | solution.py:38
  9.6 3.0 copy-start
  9.6 3.6 copy-start.2
  13.2 7.1 %copy-start.1 = (bf16[1,768,1408]{2,1,0:T(8,128)(2,1)S(1)}, bf16[1,768,1408]{2,1,0:T(8,128)(2,1)}, u32[]{:S(2)}) copy-start(bf16[1,768,1408]{2,1,0:T(8,128)(2,1)} %param.10) | copy-start | bytes 6488068
  39.2 7.3 %copy-start.5 = (bf16[768,1408]{1,0:T(8,128)(2,1)S(1)}, bf16[768,1408]{1,0:T(8,128)(2,1)}, u32[]{:S(2)}) copy-start(bf16[768,1408]{1,0:T(8,128)(2,1)} %fusion.7) | copy-start | bytes 6488068
  61.1 1.4 copy-start.7
  61.1 1.8 copy-start.8
  61.2 343.4 %all-reduce.18.cloned.1.call-start = ((), (), s32[]{:S(2)}) async-start(), calls=%async_computation.4 | async-start | bytes 139264 | tf_op jit(solution)/shard_map/psum | solution.py:44
  62.1 344.5 %all-gather.10.cloned.1.call-start = ((), (), s32[]{:S(2)}) async-start(), calls=%async_computation.6 | async-start | bytes 7208960 | tf_op jit(solution)/shard_map/all_gather | solution.py:20
  64.8 351.0 %all-gather.8.cloned.1.call-start = ((), (), s32[]{:S(2)}) async-start(), calls=%async_computation.5 | async-start | bytes 7208960 | tf_op jit(solution)/shard_map/all_gather | solution.py:20
  65.3 457.5 %all-reduce.20.cloned.1.call-start = ((), (), s32[]{:S(2)}) async-start(), calls=%async_computation.7 | async-start | bytes 11534336 | tf_op jit(solution)/shard_map/psum | solution.py:100
  269.6 137.1 %copy-start.4 = (bf16[768,1408]{1,0:T(8,128)(2,1)S(1)}, bf16[768,1408]{1,0:T(8,128)(2,1)}, u32[]{:S(2)}) copy-start(bf16[768,1408]{1,0:T(8,128)(2,1)} %fusion.6) | copy-start | bytes 6488068
  415.7 8.1 %copy-start.6 = (bf16[4,768,256]{1,2,0:T(8,128)(2,1)S(1)}, bf16[4,768,256]{1,2,0:T(8,128)(2,1)}, u32[]{:S(2)}) copy-start(bf16[4,768,256]{1,2,0:T(8,128)(2,1)} %fusion.13) | copy-start | bytes 4718596
  522.8 3.8 copy-start.3
Sparse Core Ops, SparseCore 0:
  10.5 18.4 all-gather.5
  61.3 202.6 reduce-scatter.1
  266.2 60.8 all-gather.9
  328.6 61.9 all-gather.7
Sparse Core Ops, SparseCore 1:
  66.4 338.1 all-reduce.17
  408.4 114.3 all-reduce.19
where the time goes:
time: 536 us
  waiting for transfers between devices  418 us (78%)
  other arithmetic  46.8 us (9%)
  matrix products  29.9 us (6%)
  local copies, waits for them, and re-layouts  19.1 us (4%)
  between operations  15.4 us (3%)
  blocking collectives  5.9 us (1%)
    reduce_scatter x1, waiting for transfers between devices, side_by_side(): result = lax.psum_scatter(both, axis, scatter_dimension=dim, tiled=True)  198 us
    psum x1, waiting for transfers between devices, in_one(): subtotal = lax.psum(ravelled, axis)  135 us
    psum x1, waiting for transfers between devices, per_device(): whole = lax.psum((pieces[0], pieces[1]), 'rep')  83.4 us
    dot_general x2, matrix products, project(): jnp.einsum('lkf,knf->ln', stacked, weight_block, preferred_element_type=j...  17.1 us
    reduce_sum x2, other arithmetic, causal_mix(): kernel[1] * padded[1:length + 1]  11.8 us
  transfers between devices with their start and end apart: 6, of which 3 were waited for; matrix products, arithmetic and copies ran while one was open for 12% of the time, Pallas kernels for 0%

commit v1 on v0

--- a/solution.py
+++ b/solution.py
@@ -41,7 +41,7 @@
 
 def in_one(arrays, axis):
     ravelled, at, gathered = (jnp.concatenate([a.reshape(-1) for a in arrays]), 0, [])
-    subtotal = lax.psum(ravelled, axis)
+    subtotal = jnp.sum(lax.all_gather(ravelled, axis), axis=0)
     for a in arrays:
         gathered.append(subtotal[at : at + a.size].reshape(a.shape))
         at += a.size

time: 536 us -> 594 us (1.11)
  waiting for transfers between devices: 418 us -> 470 us
    psum x1 -> x0, waiting for transfers between devices: 135 us -> none  [in_one(): subtotal = lax.psum(ravelled, axis)]
    all_gather x2, waiting for transfers between devices: 0.01 us -> 112 us  [work_in_pieces(): gathered.append(jax.vmap(apply)(lax.all_gather(section, axis), starts))]
    all_gather x0 -> x1, waiting for transfers between devices: none -> 49.2 us  [in_one(): subtotal = jnp.sum(lax.all_gather(ravelled, axis), axis=0)]
    psum x1, waiting for transfers between devices: 83.4 us -> 111 us  [per_device(): whole = lax.psum((pieces[0], pieces[1]), 'rep')]
    reduce_sum x0 -> x1, other arithmetic: none -> 6.5 us  [in_one(): subtotal = jnp.sum(lax.all_gather(ravelled, axis), axis=0)]
  transfers between devices with their start and end apart: 6 -> 6, of which waited for: 3 -> 5; matrix products, arithmetic and copies ran while one was open for 12% -> 12% of each run, Pallas kernels for 0% -> 0%
where the time goes in v1:
time: 594 us
  waiting for transfers between devices  470 us (79%)
  other arithmetic  51.7 us (9%)
  matrix products  29.9 us (5%)
  local copies, waits for them, and re-layouts  20.7 us (3%)
  between operations  14.4 us (2%)
  blocking collectives  6.72 us (1%)
    reduce_scatter x1, waiting for transfers between devices, side_by_side(): result = lax.psum_scatter(both, axis, scatter_dimension=dim, tiled=True)  197 us
    all_gather x2, waiting for transfers between devices, work_in_pieces(): gathered.append(jax.vmap(apply)(lax.all_gather(section, axis), starts))  112 us
    psum x1, waiting for transfers between devices, per_device(): whole = lax.psum((pieces[0], pieces[1]), 'rep')  111 us
    all_gather x1, waiting for transfers between devices, in_one(): subtotal = jnp.sum(lax.all_gather(ravelled, axis), axis=0)  49.2 us
    dot_general x2, matrix products, project(): jnp.einsum('lkf,knf->ln', stacked, weight_block, preferred_element_type=j...  17.1 us
  transfers between devices with their start and end apart: 6, of which 5 were waited for; matrix products, arithmetic and copies ran while one was open for 12% of the time, Pallas kernels for 0%

profile of v1, /device:TPU:1, one launch (start us, length us, event | category | flops | bytes accessed | tf_op | source)
XLA Modules:
  0.0 593.6 jit_solution(15698841519979893899)
XLA Ops:
  7.2 0.0 all-gather.9.cloned.1.call-start
  7.2 0.7 all-gather.9.cloned.1.call-update
  7.9 0.0 reduce-scatter.2.cloned.1.call-start
  8.0 0.7 dynamic-slice_convert_fusion
  8.7 0.1 slice_reduce_fusion.5
  8.8 0.0 copy-start
  8.8 0.0 copy-start.2
  8.8 3.0 bitcast_convert_fusion.2
  11.8 0.0 copy-done
  11.8 0.6 copy-done.2
  12.4 0.0 copy-start.1
  12.4 7.1 %multiply_reduce_fusion.4 = (f32[1408]{0:T(1024)S(1)}, f32[1408]{0:T(1024)S(1)}, f32[1408]{0:T(1024)S(1)}, f32[768,1408]{1,0:T(8,128)S(1)}, f32[768,1408]{1,0:T(8,128)S(1)}) fusion(f32[768,1408]{1,0:T(8,128)S(1)} %get-tuple-element.41, bf16[1,768,1408]{2,1,0:T(8,128)(2,1)S(1)} %copy-done, f32[768,1408]{1,0:T(8,128)S(1)} %get-tuple-element.42, ...), kind=kLoop, calls=%fused_computation.24 | loop fusion | flops 41086848 | bytes 21677568 | tf_op jit(solution)/shard_map/transpose(jvp())/reduce_sum | solution.py:56
  19.5 0.0 copy-done.1
  19.5 4.6 multiply_reduce_fusion.1
  24.2 2.8 broadcast_multiply_fusion.2
  27.0 4.7 fusion.6
  31.7 0.8 broadcast_multiply_fusion.5
  32.6 2.3 fusion.7
  34.9 0.0 all-gather.9.cloned.1.call-done
  34.9 3.4 copy.16
  38.3 0.0 copy-start.5
  38.3 7.3 %convolution_bitcast_fusion = f32[4,512,1408]{2,1,0:T(8,128)S(1)} fusion(bf16[768,4,512]{0,2,1:T(8,128)(2,1)S(1)} %bitcast.73, bf16[768,1408]{1,0:T(8,128)(2,1)} %fusion.6), kind=kOutput, calls=%fused_computation.1 | convolution fusion | flops 4429185024 | bytes 16842752 | tf_op jit(solution)/shard_map/nfd,nk->fdk/dot_general | solution.py:97
  45.6 0.0 copy-done.5
  45.6 5.5 convolution_bitcast_fusion.1
  51.1 9.1 %pad_maximum_fusion = f32[4,1024,1408]{2,1,0:T(8,128)} fusion(f32[4,512,1408]{2,1,0:T(8,128)S(1)} %convolution_bitcast_fusion, f32[4,512,1408]{2,1,0:T(8,128)S(1)} %convolution_bitcast_fusion.1), kind=kLoop, calls=%fused_computation | loop fusion | flops 5767168 | bytes 46137344 | tf_op jit(solution)/shard_map/concatenate | solution.py:37
  60.2 0.0 copy-start.7
  60.2 0.0 copy-start.8
  60.2 0.0 reduce-scatter.2.cloned.1.call-update
  60.3 0.0 all-gather.13.cloned.1.call-start
  60.3 1.3 copy-done.7
  61.6 0.4 copy-done.8
  62.0 1.8 fusion.14
  63.8 0.0 all-gather.13.cloned.1.call-update
  63.8 0.0 all-gather.11.cloned.1.call-start
  63.9 0.5 all-gather.11.cloned.1.call-update
  64.4 0.0 all-gather.15.cloned.1.call-start
  64.7 0.7 reshape.100
  65.4 0.0 all-gather.15.cloned.1.call-update
  65.4 0.3 all-reduce.17.cloned.1.call-start
  65.7 196.7 %reduce-scatter.2.cloned.1.call-done = f32[1,1024,1408]{2,1,0:T(8,128)} async-done(((f32[4,1024,1408]{2,1,0:T(8,128)}), f32[1,1024,1408]{2,1,0:T(8,128)}) %reduce-scatter.2.cloned.1.call-update) | async-done | bytes 5767184 | tf_op jit(solution)/shard_map/reduce_scatter | solution.py:38
  262.4 5.6 fusion.18
  268.0 0.0 copy-start.4
  268.0 0.0 all-reduce.17.cloned.1.call-update
  268.0 57.6 %all-gather.13.cloned.1.call-done = bf16[8,256,1408]{2,1,0:T(8,128)(2,1)} async-done(((bf16[2,256,1408]{2,1,0:T(8,128)(2,1)}), bf16[8,256,1408]{2,1,0:T(8,128)(2,1)}) %all-gather.13.cloned.1.call-update) | async-done | bytes 5767184 | tf_op jit(solution)/shard_map/all_gather | solution.py:20
  325.5 0.0 copy-done.4
  325.5 9.1 %fusion.13 = bf16[4,768,256]{1,2,0:T(8,128)(2,1)} fusion(bf16[4,2,256,1408]{3,2,1,0:T(8,128)(2,1)} %bitcast.81, bf16[768,1,1408]{2,0,1:T(8,128)(2,1)S(1)} %bitcast.75, bf16[768,1,1408]{2,0,1:T(8,128)(2,1)} %bitcast.77), kind=kOutput, calls=%fused_computation.51 | convolution fusion | flops 4438622208 | bytes 11665408 | tf_op jit(solution)/shard_map/vmap(lkf,knf->ln)/dot_general | solution.py:82
  334.6 54.3 %all-gather.11.cloned.1.call-done = bf16[8,256,1408]{2,1,0:T(8,128)(2,1)} async-done(((bf16[2,256,1408]{2,1,0:T(8,128)(2,1)}), bf16[8,256,1408]{2,1,0:T(8,128)(2,1)}) %all-gather.11.cloned.1.call-update) | async-done | bytes 5767184 | tf_op jit(solution)/shard_map/all_gather | solution.py:20
  388.9 0.0 copy-start.6
  388.9 8.1 %fusion.12 = bf16[4,768,256]{1,2,0:T(8,128)(2,1)S(1)} fusion(bf16[4,2,256,1408]{3,2,1,0:T(8,128)(2,1)} %bitcast.82, bf16[768,1,1408]{2,0,1:T(8,128)(2,1)S(1)} %bitcast.76, bf16[768,1,1408]{2,0,1:T(8,128)(2,1)} %bitcast.78), kind=kOutput, calls=%fused_computation.50 | convolution fusion | flops 4438622208 | bytes 11665408 | tf_op jit(solution)/shard_map/vmap(lkf,knf->ln)/dot_general | solution.py:82
  397.0 0.0 copy-done.6
  397.0 0.2 maximum_bitcast_fusion.1
  397.2 2.4 convert_element_type.47
  399.7 2.3 copy.14
  401.9 6.7 %all_to_all.5 = bf16[2,384,2048]{1,2,0:T(8,128)(2,1)S(1)} all-to-all(bf16[2,384,2048]{1,2,0:T(8,128)(2,1)S(1)} %copy.14), channel_id=1, replica_groups=mesh['rep'=16,'fs'=4,'tp'=2] {'tp'}, dimensions={0} | all-to-all | bytes 6291456 | tf_op jit(solution)/shard_map/all_to_all | solution.py:31
  408.7 2.2 reduce_sum.76
  410.8 2.6 copy.17
  413.4 49.2 %all-gather.15.cloned.1.call-done = f32[128,1,16896]{2,1,0:T(1,128)} async-done(((f32[1,1,16896]{2,1,0:T(1,128)}), f32[128,1,16896]{2,1,0:T(1,128)}) %all-gather.15.cloned.1.call-update) | async-done | bytes 8650768 | tf_op jit(solution)/shard_map/all_gather | solution.py:44
  462.6 6.5 %reduce_sum.86 = f32[16896]{0:T(1024)S(1)} reduce(f32[128,1,16896]{2,1,0:T(1,128)} %all-gather.15.cloned.1.call-done, f32[]{:T(128)} %constant.8.clone.1), dimensions={0,1}, to_apply=%region_10.11 | reduce | flops 2145792 | bytes 8718340 | tf_op jit(solution)/shard_map/reduce_sum | solution.py:44
  469.1 0.6 mul.244
  469.8 0.6 mul.246
  470.4 110.8 %all-reduce.17.cloned.1.call-done = (f32[1,512,1408]{2,1,0:T(8,128)}, f32[1,512,1408]{2,1,0:T(8,128)}) async-done(((f32[1,512,1408]{2,1,0:T(8,128)}, f32[1,512,1408]{2,1,0:T(8,128)}), (f32[1,512,1408]{2,1,0:T(8,128)}, f32[1,512,1408]{2,1,0:T(8,128)})) %all-reduce.17.cloned.1.call-update) | async-done | bytes 5767184 | tf_op jit(solution)/shard_map/psum | solution.py:100
  581.2 3.8 multiply_bitcast_fusion.1
  585.0 0.0 copy-done.3
  585.0 1.8 multiply_bitcast_fusion
  (16 shorter events, 0.2 us)
Async XLA Ops:
  7.2 27.7 %all-gather.9.cloned.1.call-start = ((), (), s32[]{:S(2)}) async-start(), calls=%async_computation.2 | async-start | bytes 4718592 | tf_op jit(solution)/shard_map/all_gather | solution.py:93
  7.9 254.5 %reduce-scatter.2.cloned.1.call-start = ((), (), s32[]{:S(2)}) async-start(), calls=%async_computation.3 | async-start | bytes 28835840 | tf_op jit(solution)/shard_map/reduce_scatter | solution.py:38
  8.8 3.0 copy-start
  8.8 3.6 copy-start.2
  12.4 7.1 %copy-start.1 = (bf16[1,768,1408]{2,1,0:T(8,128)(2,1)S(1)}, bf16[1,768,1408]{2,1,0:T(8,128)(2,1)}, u32[]{:S(2)}) copy-start(bf16[1,768,1408]{2,1,0:T(8,128)(2,1)} %param.10) | copy-start | bytes 6488068
  38.3 7.3 %copy-start.5 = (bf16[768,1408]{1,0:T(8,128)(2,1)S(1)}, bf16[768,1408]{1,0:T(8,128)(2,1)}, u32[]{:S(2)}) copy-start(bf16[768,1408]{1,0:T(8,128)(2,1)} %fusion.7) | copy-start | bytes 6488068
  60.2 1.4 copy-start.7
  60.2 1.8 copy-start.8
  60.3 265.3 %all-gather.13.cloned.1.call-start = ((), (), s32[]{:S(2)}) async-start(), calls=%async_computation.5 | async-start | bytes 7208960 | tf_op jit(solution)/shard_map/all_gather | solution.py:20
  63.8 325.1 %all-gather.11.cloned.1.call-start = ((), (), s32[]{:S(2)}) async-start(), calls=%async_computation.4 | async-start | bytes 7208960 | tf_op jit(solution)/shard_map/all_gather | solution.py:20
  64.4 398.2 %all-gather.15.cloned.1.call-start = ((), (), s32[]{:S(2)}) async-start(), calls=%async_computation.6 | async-start | bytes 8718336 | tf_op jit(solution)/shard_map/all_gather | solution.py:44
  65.4 515.7 %all-reduce.17.cloned.1.call-start = ((), (), s32[]{:S(2)}) async-start(), calls=%async_computation.7 | async-start | bytes 11534336 | tf_op jit(solution)/shard_map/psum | solution.py:100
  268.0 57.6 %copy-start.4 = (bf16[768,1408]{1,0:T(8,128)(2,1)S(1)}, bf16[768,1408]{1,0:T(8,128)(2,1)}, u32[]{:S(2)}) copy-start(bf16[768,1408]{1,0:T(8,128)(2,1)} %fusion.6) | copy-start | bytes 6488068
  388.9 8.1 %copy-start.6 = (bf16[4,768,256]{1,2,0:T(8,128)(2,1)S(1)}, bf16[4,768,256]{1,2,0:T(8,128)(2,1)}, u32[]{:S(2)}) copy-start(bf16[4,768,256]{1,2,0:T(8,128)(2,1)} %fusion.13) | copy-start | bytes 4718596
  581.2 3.8 copy-start.3
Sparse Core Ops, SparseCore 0:
  9.6 18.4 all-gather.8
  60.4 201.9 reduce-scatter.1
  264.6 60.8 all-gather.12
  327.1 61.8 all-gather.10
  391.8 70.8 all-gather.14
  466.5 114.6 all-reduce.16
